TPU v7x, 32 devices: a whole 2x2x4 slice. The times are simulated.
32 devices in a mesh: sp: 4 (over z), fs: 4 (over y, x), tp: 2 (over core).
Axes of the slice: x: 2, y: 2, z: 4, core: 2. Of those that a mesh axis runs over, the one named last changes fastest.
Arguments:
- tokens: bfloat16 [2048, 2048], P(('fs', 'sp'), 'tp'), parts along dimension 0, may hold values from -6 to 6
- norm_gain: float32 [2048], replicated, may hold values from 0.1 to 1.9
- w_recept: bfloat16 [2048, 1024], P('sp', 'tp'), may hold values from -0.125 to 0.125
- w_key_a: bfloat16 [2048, 1024], P('sp', 'tp'), may hold values from -0.125 to 0.125
- w_value_a: bfloat16 [2048, 1024], P('sp', 'tp'), may hold values from -0.125 to 0.125
- w_gate_a: bfloat16 [2048, 1024], P('sp', 'tp'), may hold values from -0.125 to 0.125
- decay_down_weight: bfloat16 [2048, 64], replicated, may hold values from -0.125 to 0.125
- decay_up_weight: bfloat16 [64, 1024], P(None, 'tp'), may hold values from -0.75 to 0.75
- rate_down_weight: bfloat16 [2048, 64], replicated, may hold values from -0.125 to 0.125
- rate_up_weight: bfloat16 [64, 1024], P(None, 'tp'), may hold values from -0.75 to 0.75
- decay_base: float32 [1024], P('tp'), may hold values from -12 to -2.5
- rate_base: float32 [1024], P('tp'), may hold values from -12 to 1
- rate_shift: float32 [2048, 16], P(('fs', 'sp'), 'tp'), parts along dimension 0, may hold values from 0 to 1.39
- jolts: float32 [2048, 16], P(('fs', 'sp'), 'tp'), parts along dimension 0, may hold values from 0 to 0.69
- group_gain: float32 [1024], P('tp'), may hold values from 0.1 to 1.9
- w_query_b: bfloat16 [2048, 1024], P('sp', 'tp'), may hold values from -0.125 to 0.125
- w_key_b: bfloat16 [2048, 1024], P('sp', 'tp'), may hold values from -0.125 to 0.125
- w_value_b: bfloat16 [2048, 1024], P('sp', 'tp'), may hold values from -0.125 to 0.125
- w_gate_b: bfloat16 [2048, 1024], P('sp', 'tp'), may hold values from -0.125 to 0.125
- score_offset: float32 [8], P('tp'), may hold values from -12 to -1
- w_out_a: bfloat16 [1024, 2048], P('tp'), may hold values from -0.125 to 0.125
- w_out_b: bfloat16 [1024, 2048], P('tp'), may hold values from -0.125 to 0.125
Outputs:
- mixed: bfloat16 [2048, 2048], P(('fs', 'sp', 'tp')), parts along dimension 0
- row_log: float32 [2048, 8], P(('fs', 'sp'), 'tp'), parts along dimension 0
There are 4 independent parts, one for each index of `fs`. A program takes and returns all parts, laid end to end along the dimension named above; an argument that names none is the same for every part. Nothing has to cross between parts.
All inputs are finite; a program needn't handle non-finite values.
Results may differ from a plain program's by a relative error of at most 0.02.
Values may be sent and summed in bfloat16 or wider, within the bound.
A program may use at most 64 MiB of HBM per device.

v0:
```python
import jax
import jax.numpy as jnp
from jax import lax
from jax.sharding import PartitionSpec as P

HEAD_A = 64
HEAD_B = 128


highest = lax.Precision.HIGHEST


def entering_2(value, axis, combine, identity):
    devices, index = (lax.axis_size(axis), lax.axis_index(axis))
    everything = jax.tree.map(
        lambda part, kind: lax.all_gather(part.astype(kind), axis),
        value,
        (jnp.bfloat16, jnp.bfloat16),
    )
    start = jax.tree.map(
        lambda part, zero: jnp.broadcast_to(jnp.asarray(zero, part.dtype), part.shape),
        value,
        identity,
    )

    def lap(k, before):
        reached = k < index
        new = combine(
            before, jax.tree.map(lambda part, own: part[k].astype(own.dtype), everything, value)
        )
        return jax.tree.map(lambda a, b: jnp.where(reached, a, b), new, before)

    return lax.fori_loop(0, devices, lap, start)


def combine_states(earlier, follower):
    joined = jnp.einsum("hij,hjk->hik", earlier[0], follower[0], precision=highest)
    carried = jnp.einsum("hij,hjk->hik", earlier[1], follower[0], precision=highest) + follower[1]
    return (joined, carried)


def block_pass(stacked, pieces):
    recept_c, logs_step, keys_c, values_c, unit_c, mixing_c = pieces
    block_len = recept_c.shape[0]
    totals = jnp.cumsum(logs_step, axis=0)
    preceding = jnp.concatenate([jnp.zeros_like(totals[:1]), totals[:-1]], axis=0)
    steering = unit_c * mixing_c
    places_here = jnp.arange(block_len, dtype=jnp.int32)
    below_diag = (places_here[:, None] > places_here[None, :])[:, :, None, None]
    fading = jnp.where(
        below_diag, jnp.exp(jnp.where(below_diag, preceding[:, None] - totals[None, :], 0.0)), 0.0
    )
    unit_fade = fading * unit_c[:, None]
    weigh_keys = jnp.einsum("tjhc,jhc->htj", unit_fade, keys_c, precision=highest)
    weigh_steer = jnp.einsum("tjhc,jhc->htj", unit_fade, steering, precision=highest)
    read_fade = fading * (recept_c * jnp.exp(logs_step))[:, None]
    diagonal = jnp.eye(block_len, dtype=jnp.float32)
    read_keys = (
        jnp.einsum("tjhc,jhc->htj", read_fade, keys_c, precision=highest)
        + diagonal * jnp.sum(recept_c * keys_c, axis=2).T[:, :, None]
    )
    read_steer = (
        jnp.einsum("tjhc,jhc->htj", read_fade, steering, precision=highest)
        + diagonal * jnp.sum(recept_c * steering, axis=2).T[:, :, None]
    )
    values_wide = jnp.concatenate([jnp.zeros_like(values_c), values_c], axis=2)
    entering = jnp.einsum("thc,hrc->htr", unit_c * jnp.exp(preceding), stacked, precision=highest)
    entering = entering + jnp.einsum("htj,jhr->htr", weigh_keys, values_wide, precision=highest)
    removal = jax.scipy.linalg.solve_triangular(
        weigh_steer + diagonal, entering, lower=True, unit_diagonal=True
    )
    readout = jnp.einsum("thc,hrc->htr", recept_c * jnp.exp(totals), stacked, precision=highest)
    readout = readout + jnp.einsum("htj,jhr->htr", read_keys, values_wide, precision=highest)
    readout = readout - jnp.einsum("htj,hjr->htr", read_steer, removal, precision=highest)
    tail_fade = jnp.exp(totals[-1][None] - totals)
    closing = stacked * jnp.exp(totals[-1])[:, None, :]
    closing = closing + jnp.einsum(
        "jhr,jhc->hrc", values_wide, keys_c * tail_fade, precision=highest
    )
    closing = closing - jnp.einsum("hjr,jhc->hrc", removal, steering * tail_fade, precision=highest)
    return (closing, jnp.transpose(readout, (1, 0, 2)))


def local(
    tokens,
    norm_gain,
    w_recept,
    w_key_a,
    w_value_a,
    w_gate_a,
    decay_down_weight,
    decay_up_weight,
    rate_down_weight,
    rate_up_weight,
    decay_base,
    rate_base,
    rate_shift,
    jolts,
    group_gain,
    w_query_b,
    w_key_b,
    w_value_b,
    w_gate_b,
    score_offset,
    w_out_a,
    w_out_b,
):
    gathered = lax.all_gather(tokens, "tp", axis=1, tiled=True)
    floats = gathered.astype(jnp.float32)
    normed = (
        floats * lax.rsqrt(jnp.mean(floats * floats, axis=1, keepdims=True) + 1e-06) * norm_gain
    ).astype(jnp.bfloat16)
    row_count = normed.shape[0]
    matrices = (w_recept, w_key_a, w_value_a, w_gate_a, w_query_b, w_key_b, w_value_b, w_gate_b)
    portions = (
        lax.all_gather(matrices[0], "sp", axis=0, tiled=True),
        lax.all_gather(matrices[1], "sp", axis=0, tiled=True),
        lax.all_gather(matrices[2], "sp", axis=0, tiled=True),
        lax.all_gather(matrices[3], "sp", axis=0, tiled=True),
        lax.all_gather(matrices[4], "sp", axis=0, tiled=True),
        lax.all_gather(matrices[5], "sp", axis=0, tiled=True),
        lax.all_gather(matrices[6], "sp", axis=0, tiled=True),
        lax.all_gather(matrices[7], "sp", axis=0, tiled=True),
    )
    projected = tuple(
        (jnp.dot(normed, portion, preferred_element_type=jnp.float32) for portion in portions)
    )
    recept, keys_a, values_a, gate_a, query_b, keys_b, values_b, gate_b = [
        summed.astype(jnp.bfloat16) for summed in projected
    ]
    heads_a = recept.shape[1] // HEAD_A
    decay_low = jnp.tanh(
        jnp.dot(normed, decay_down_weight, preferred_element_type=jnp.float32)
    ).astype(jnp.bfloat16)
    rate_low = jnp.dot(normed, rate_down_weight, preferred_element_type=jnp.float32).astype(
        jnp.bfloat16
    )
    preact = (
        decay_base
        + jnp.dot(decay_low, decay_up_weight, preferred_element_type=jnp.float32)
        + jnp.repeat(rate_shift, HEAD_A, axis=1)
    )
    log_decay = -jnp.exp(-jax.nn.softplus(-preact) - 0.5) - jnp.repeat(jolts, HEAD_A, axis=1)
    mixing = jax.nn.sigmoid(
        rate_base + jnp.dot(rate_low, rate_up_weight, preferred_element_type=jnp.float32)
    )

    def split_heads(matrix):
        return matrix.astype(jnp.float32).reshape(row_count, heads_a, HEAD_A)

    keys_heads = split_heads(keys_a)
    unit_keys = keys_heads * lax.rsqrt(
        jnp.sum(keys_heads * keys_heads, axis=2, keepdims=True) + 1e-06
    )
    block_len = min(32, row_count)
    block_count = row_count // block_len

    def to_blocks(matrix):
        return matrix.reshape(block_count, block_len, heads_a, HEAD_A)

    inputs = tuple(
        (
            to_blocks(matrix)
            for matrix in (
                split_heads(recept),
                log_decay.reshape(row_count, heads_a, HEAD_A),
                keys_heads,
                split_heads(values_a),
                unit_keys,
                mixing.reshape(row_count, heads_a, HEAD_A),
            )
        )
    )
    identity = jnp.broadcast_to(jnp.eye(HEAD_A, dtype=jnp.float32), (heads_a, HEAD_A, HEAD_A))
    zeros_state = jnp.zeros((heads_a, HEAD_A, HEAD_A), jnp.float32)
    closing, readout = lax.scan(
        block_pass, jnp.concatenate([identity, zeros_state], axis=1), inputs
    )
    readout = readout.reshape(row_count, heads_a, 2 * HEAD_A)
    prefix = entering_2(
        (closing[:, :HEAD_A], closing[:, HEAD_A:]), "sp", combine_states, (identity, zeros_state)
    )
    outputs_a = readout[:, :, HEAD_A:] + jnp.einsum(
        "hvk,thk->thv", prefix[1], readout[:, :, :HEAD_A], precision=highest
    )
    centered = outputs_a - jnp.mean(outputs_a, axis=2, keepdims=True)
    normal_a = centered * lax.rsqrt(jnp.mean(centered * centered, axis=2, keepdims=True) + 0.00064)
    mixed_a = (
        normal_a.reshape(row_count, -1) * group_gain * jax.nn.silu(gate_a.astype(jnp.float32))
    ).astype(jnp.bfloat16)
    heads_b = query_b.shape[1] // HEAD_B
    own_index = lax.axis_index("sp")
    places = jnp.arange(row_count, dtype=jnp.int32)
    query_place = own_index * row_count + places
    query_heads = query_b.reshape(row_count, heads_b, HEAD_B)
    factor = HEAD_B ** (-0.5)
    paired = jnp.stack(
        [keys_b.reshape(row_count, heads_b, HEAD_B), values_b.reshape(row_count, heads_b, HEAD_B)]
    )

    def attend(running, paired_piece, source):
        attended, weight_sum, survive = running
        scores = (
            jnp.einsum(
                "qhd,khd->hqk", query_heads, paired_piece[0], preferred_element_type=jnp.float32
            )
            * factor
            + score_offset[:, None, None]
        )
        causal = (source * row_count + places)[None, None, :] < query_place[None, :, None]
        keep_log = jnp.where(causal, jax.nn.log_sigmoid(-scores), 0.0)
        later_sum = (
            jnp.flip(jnp.cumsum(jnp.flip(keep_log, 2), axis=2), 2) - keep_log + survive[:, :, None]
        )
        weights = jnp.where(causal, jnp.exp(jax.nn.log_sigmoid(scores) + later_sum), 0.0)
        attended = attended + jnp.einsum(
            "hqk,khd->qhd",
            weights.astype(jnp.bfloat16),
            paired_piece[1],
            preferred_element_type=jnp.float32,
        )
        return (
            attended,
            weight_sum + jnp.sum(weights, axis=2),
            survive + jnp.sum(keep_log, axis=2),
        )

    empty_b = (
        jnp.zeros((row_count, heads_b, HEAD_B), jnp.float32),
        jnp.zeros((heads_b, row_count), jnp.float32),
        jnp.zeros((heads_b, row_count), jnp.float32),
    )
    running = attend(empty_b, paired, own_index)
    all_pairs = lax.all_gather(paired[None], "sp", axis=0, tiled=True)

    def visit_piece(rounds, holding):
        source = own_index - rounds
        chosen = lax.dynamic_index_in_dim(all_pairs, jnp.maximum(source, 0), 0, False)
        return lax.cond(
            source >= 0, lambda kept: attend(kept, chosen, source), lambda kept: kept, holding
        )

    running = lax.fori_loop(1, lax.axis_size("sp"), visit_piece, running)
    mixed_b = (running[0].reshape(row_count, -1) * jax.nn.silu(gate_b.astype(jnp.float32))).astype(
        jnp.bfloat16
    )
    row_log = jnp.log(jnp.maximum(running[1].T, 0.01))
    mixed = lax.psum_scatter(
        (
            jnp.dot(mixed_a, w_out_a, preferred_element_type=jnp.float32)
            + jnp.dot(mixed_b, w_out_b, preferred_element_type=jnp.float32)
        ).astype(jnp.bfloat16),
        "tp",
        scatter_dimension=0,
        tiled=True,
    )
    return (mixed, row_log)


def solution(mesh):
    in_specs = (
        P(("fs", "sp"), "tp"),
        P(),
        P("sp", "tp"),
        P("sp", "tp"),
        P("sp", "tp"),
        P("sp", "tp"),
        P(),
        P(None, "tp"),
        P(),
        P(None, "tp"),
        P("tp"),
        P("tp"),
        P(("fs", "sp"), "tp"),
        P(("fs", "sp"), "tp"),
        P("tp"),
        P("sp", "tp"),
        P("sp", "tp"),
        P("sp", "tp"),
        P("sp", "tp"),
        P("tp"),
        P("tp", None),
        P("tp", None),
    )
    out_specs = (P(("fs", "sp", "tp"), None), P(("fs", "sp"), "tp"))
    return jax.shard_map(local, mesh=mesh, in_specs=in_specs, out_specs=out_specs, check_vma=False)
```

profile of v0, /device:TPU:0, one launch (start us, length us, event | category | flops | bytes accessed | tf_op | source)
XLA Modules:
  0.0 745.0 jit_solution(5044790443261289042)
XLA Ops:
  14.5 43.5 %all-gather.25.cloned.1.call-done = bf16[2048,512]{1,0:T(8,128)(2,1)} async-done(((bf16[512,512]{1,0:T(8,128)(2,1)}), bf16[2048,512]{1,0:T(8,128)(2,1)}) %all-gather.25.cloned.1.call-update) | async-done | bytes 2097168 | tf_op jit(solution)/shard_map/all_gather | solution.py:121
  60.8 43.2 %all-gather.21.cloned.1.call-done = bf16[2048,512]{1,0:T(8,128)(2,1)} async-done(((bf16[512,512]{1,0:T(8,128)(2,1)}), bf16[2048,512]{1,0:T(8,128)(2,1)}) %all-gather.21.cloned.1.call-update) | async-done | bytes 2097168 | tf_op jit(solution)/shard_map/all_gather | solution.py:122
  115.5 34.6 %all-gather.23.cloned.1.call-done = bf16[2048,512]{1,0:T(8,128)(2,1)} async-done(((bf16[512,512]{1,0:T(8,128)(2,1)}), bf16[2048,512]{1,0:T(8,128)(2,1)}) %all-gather.23.cloned.1.call-update) | async-done | bytes 2097168 | tf_op jit(solution)/shard_map/all_gather | solution.py:120
  156.4 39.7 %all-gather.15.cloned.1.call-done = bf16[2048,512]{1,0:T(8,128)(2,1)} async-done(((bf16[512,512]{1,0:T(8,128)(2,1)}), bf16[2048,512]{1,0:T(8,128)(2,1)}) %all-gather.15.cloned.1.call-update) | async-done | bytes 2097168 | tf_op jit(solution)/shard_map/all_gather | solution.py:117
  199.4 42.6 %all-gather.13.cloned.1.call-done = bf16[2048,512]{1,0:T(8,128)(2,1)} async-done(((bf16[512,512]{1,0:T(8,128)(2,1)}), bf16[2048,512]{1,0:T(8,128)(2,1)}) %all-gather.13.cloned.1.call-update) | async-done | bytes 2097168 | tf_op jit(solution)/shard_map/all_gather | solution.py:118
  244.9 42.9 %all-gather.17.cloned.1.call-done = bf16[2048,512]{1,0:T(8,128)(2,1)} async-done(((bf16[512,512]{1,0:T(8,128)(2,1)}), bf16[2048,512]{1,0:T(8,128)(2,1)}) %all-gather.17.cloned.1.call-update) | async-done | bytes 2097168 | tf_op jit(solution)/shard_map/all_gather | solution.py:116
  292.9 363.7 %while.44 = (s32[]{:T(128)}, f32[8,128,64]{1,2,0:T(8,128)S(1)}, f32[4,32,8,128]{3,2,1,0:T(8,128)}, f32[4,32,8,64]{3,2,1,0:T(8,128)}, f32[4,32,8,64]{3,2,1,0:T(8,...) while((s32[]{:T(128)}, f32[8,128,64]{1,2,0:T(8,128)S(1)}, ...), condition=%wide.region_6.7_spmd, body=%wide.region_2.6_spmd.sunk | while | flops 179844640 | bytes 36615644 | solution.py:176
  334.1 11.4 %fusion.238 = f32[8,32,1,32]{3,2,1,0:T(1,128)} fusion(f32[32,32,8,64]{3,2,1,0:T(8,128)} %get-tuple-element.734, f32[32,8,64,1]{2,1,0,3:T(8,128)S(1)} %bitcast.217), kind=kOutput, calls=%fused_computation.11.clone.1 | convolution fusion | flops 6291456 | bytes 2195456 | tf_op jit(solution)/shard_map/while/body/eval_jaxpr/tjhc,jhc->htj/dot_general | solution.py:55
  348.7 21.0 %custom-call.7 = f32[8,1,32,32]{2,3,1,0:T(8,128)} custom-call(f32[8,1,32,32]{3,2,1,0:T(8,128)} %fusion.240), custom_call_target="InvertDiagBlocksLowerTriangular" | custom-call | tf_op jit(solution)/shard_map/while/body/eval_jaxpr/jit(_solve_triangular)/vmap()/triangular_solve | solution.py:69
  369.7 11.1 %fusion.236 = f32[8,32,1,32]{3,2,1,0:T(1,128)S(1)} fusion(f32[32,32,8,64]{3,2,1,0:T(8,128)} %get-tuple-element.734, f32[32,8,64,1]{2,1,0,3:T(8,128)S(1)} %get-tuple-element.735), kind=kOutput, calls=%fused_computation.9.clone.1 | convolution fusion | flops 6291456 | bytes 2195456 | tf_op jit(solution)/shard_map/while/body/eval_jaxpr/tjhc,jhc->htj/dot_general | solution.py:54
  382.1 8.6 %fusion.242 = f32[8,32,1,32]{3,2,1,0:T(1,128)S(1)} fusion(f32[32,32,8,64]{3,2,1,0:T(8,128)S(1)} %copy-done.2, f32[32,8,64,1]{2,1,0,3:T(8,128)S(1)} %bitcast.218), kind=kOutput, calls=%fused_computation.5.clone.1 | convolution fusion | flops 6291456 | bytes 2195456 | tf_op jit(solution)/shard_map/while/body/eval_jaxpr/tjhc,jhc->htj/dot_general | solution.py:63
  420.5 11.4 %fusion.238 = f32[8,32,1,32]{3,2,1,0:T(1,128)} fusion(f32[32,32,8,64]{3,2,1,0:T(8,128)} %get-tuple-element.734, f32[32,8,64,1]{2,1,0,3:T(8,128)S(1)} %bitcast.217), kind=kOutput, calls=%fused_computation.11.clone.1 | convolution fusion | flops 6291456 | bytes 2195456 | tf_op jit(solution)/shard_map/while/body/eval_jaxpr/tjhc,jhc->htj/dot_general | solution.py:55
  435.2 21.0 %custom-call.7 = f32[8,1,32,32]{2,3,1,0:T(8,128)} custom-call(f32[8,1,32,32]{3,2,1,0:T(8,128)} %fusion.240), custom_call_target="InvertDiagBlocksLowerTriangular" | custom-call | tf_op jit(solution)/shard_map/while/body/eval_jaxpr/jit(_solve_triangular)/vmap()/triangular_solve | solution.py:69
  456.2 11.0 %fusion.236 = f32[8,32,1,32]{3,2,1,0:T(1,128)S(1)} fusion(f32[32,32,8,64]{3,2,1,0:T(8,128)} %get-tuple-element.734, f32[32,8,64,1]{2,1,0,3:T(8,128)S(1)} %get-tuple-element.735), kind=kOutput, calls=%fused_computation.9.clone.1 | convolution fusion | flops 6291456 | bytes 2195456 | tf_op jit(solution)/shard_map/while/body/eval_jaxpr/tjhc,jhc->htj/dot_general | solution.py:54
  506.9 11.4 %fusion.238 = f32[8,32,1,32]{3,2,1,0:T(1,128)} fusion(f32[32,32,8,64]{3,2,1,0:T(8,128)} %get-tuple-element.734, f32[32,8,64,1]{2,1,0,3:T(8,128)S(1)} %bitcast.217), kind=kOutput, calls=%fused_computation.11.clone.1 | convolution fusion | flops 6291456 | bytes 2195456 | tf_op jit(solution)/shard_map/while/body/eval_jaxpr/tjhc,jhc->htj/dot_general | solution.py:55
  521.5 21.0 %custom-call.7 = f32[8,1,32,32]{2,3,1,0:T(8,128)} custom-call(f32[8,1,32,32]{3,2,1,0:T(8,128)} %fusion.240), custom_call_target="InvertDiagBlocksLowerTriangular" | custom-call | tf_op jit(solution)/shard_map/while/body/eval_jaxpr/jit(_solve_triangular)/vmap()/triangular_solve | solution.py:69
  542.6 11.0 %fusion.236 = f32[8,32,1,32]{3,2,1,0:T(1,128)S(1)} fusion(f32[32,32,8,64]{3,2,1,0:T(8,128)} %get-tuple-element.734, f32[32,8,64,1]{2,1,0,3:T(8,128)S(1)} %get-tuple-element.735), kind=kOutput, calls=%fused_computation.9.clone.1 | convolution fusion | flops 6291456 | bytes 2195456 | tf_op jit(solution)/shard_map/while/body/eval_jaxpr/tjhc,jhc->htj/dot_general | solution.py:54
  593.2 11.4 %fusion.238 = f32[8,32,1,32]{3,2,1,0:T(1,128)} fusion(f32[32,32,8,64]{3,2,1,0:T(8,128)} %get-tuple-element.734, f32[32,8,64,1]{2,1,0,3:T(8,128)S(1)} %bitcast.217), kind=kOutput, calls=%fused_computation.11.clone.1 | convolution fusion | flops 6291456 | bytes 2195456 | tf_op jit(solution)/shard_map/while/body/eval_jaxpr/tjhc,jhc->htj/dot_general | solution.py:55
  607.9 21.0 %custom-call.7 = f32[8,1,32,32]{2,3,1,0:T(8,128)} custom-call(f32[8,1,32,32]{3,2,1,0:T(8,128)} %fusion.240), custom_call_target="InvertDiagBlocksLowerTriangular" | custom-call | tf_op jit(solution)/shard_map/while/body/eval_jaxpr/jit(_solve_triangular)/vmap()/triangular_solve | solution.py:69
  628.9 11.0 %fusion.236 = f32[8,32,1,32]{3,2,1,0:T(1,128)S(1)} fusion(f32[32,32,8,64]{3,2,1,0:T(8,128)} %get-tuple-element.734, f32[32,8,64,1]{2,1,0,3:T(8,128)S(1)} %get-tuple-element.735), kind=kOutput, calls=%fused_computation.9.clone.1 | convolution fusion | flops 6291456 | bytes 2195456 | tf_op jit(solution)/shard_map/while/body/eval_jaxpr/tjhc,jhc->htj/dot_general | solution.py:54
  662.8 16.0 %all-gather = bf16[32,64,64]{2,1,0:T(8,128)(2,1)} all-gather(bf16[8,64,64]{2,1,0:T(8,128)(2,1)} %get-tuple-element.571), channel_id=2, replica_groups=mesh['sp'=4,'fs'=4,'tp'=2] {'sp'}, dimensions={0}, use_global_device_ids=true | all-gather | bytes 327680 | tf_op jit(solution)/shard_map/all_gather | solution.py:16
  678.8 16.2 %all-gather.1 = bf16[32,64,64]{2,1,0:T(8,128)(2,1)} all-gather(bf16[8,64,64]{2,1,0:T(8,128)(2,1)S(1)} %get-tuple-element.570), channel_id=3, replica_groups=mesh['sp'=4,'fs'=4,'tp'=2] {'sp'}, dimensions={0}, use_global_device_ids=true | all-gather | bytes 327680 | tf_op jit(solution)/shard_map/all_gather | solution.py:16
  695.0 9.3 %while.46 = (s32[]{:T(128)}, f32[8,64,64]{1,2,0:T(8,128)S(1)}, s32[]{:T(128)}, bf16[4,8,64,64]{3,2,1,0:T(8,128)(2,1)}, bf16[4,8,64,64]{3,2,1,0:T(8,128)(2,1)}, /*index=5*/s32[]{:T(128)}, s32[]{:T(128)}) while((s32[]{:T(128)}, f32[8,64,64]{1,2,0:T(8,128)S(1)}, s32[]{:T(128)}, bf16[4,8,64,64]{3,2,1,0:T(8,128)(2,1)}, ...), condition=%wide.region_8.9_spmd.clone, body=%wide.region_7.8_spmd.clone.sunk | while | flops 25329668 | bytes 1443939 | solution.py:33
  715.5 22.3 %reduce-scatter.2.cloned.1.call-done = bf16[64,2048]{1,0:T(8,128)(2,1)} async-done(((bf16[128,2048]{1,0:T(8,128)(2,1)}), bf16[64,2048]{1,0:T(8,128)(2,1)}) %reduce-scatter.2.cloned.1.call-update) | async-done | bytes 262160 | tf_op jit(solution)/shard_map/reduce_scatter | solution.py:248
  (305 shorter events, 227.9 us)
Async XLA Ops:
  7.2 699.8 %copy-start = (bf16[512,2048]{1,0:T(8,128)(2,1)S(1)}, bf16[512,2048]{1,0:T(8,128)(2,1)}, u32[]{:S(2)}) copy-start(bf16[512,2048]{1,0:T(8,128)(2,1)} %param.50) | copy-start | bytes 6291460
  7.2 50.8 %all-gather.25.cloned.1.call-start = ((), (), s32[]{:S(2)}) async-start(), calls=%async_computation.7 | async-start | bytes 2621440 | tf_op jit(solution)/shard_map/all_gather | solution.py:121
  7.9 96.1 %all-gather.21.cloned.1.call-start = ((), (), s32[]{:S(2)}) async-start(), calls=%async_computation.5 | async-start | bytes 2621440 | tf_op jit(solution)/shard_map/all_gather | solution.py:122
  8.7 49.3 %copy-start.11 = (f32[2048]{0:T(1024)S(1)}, f32[2048]{0:T(1024)}, u32[]{:S(2)}) copy-start(f32[2048]{0:T(1024)} %param.31) | copy-start | bytes 24580
  8.7 141.4 %all-gather.23.cloned.1.call-start = ((), (), s32[]{:S(2)}) async-start(), calls=%async_computation.6 | async-start | bytes 2621440 | tf_op jit(solution)/shard_map/all_gather | solution.py:120
  9.4 186.6 %all-gather.15.cloned.1.call-start = ((), (), s32[]{:S(2)}) async-start(), calls=%async_computation.2 | async-start | bytes 2621440 | tf_op jit(solution)/shard_map/all_gather | solution.py:117
  10.0 231.9 %all-gather.13.cloned.1.call-start = ((), (), s32[]{:S(2)}) async-start(), calls=%async_computation.1 | async-start | bytes 2621440 | tf_op jit(solution)/shard_map/all_gather | solution.py:118
  10.6 277.3 %all-gather.17.cloned.1.call-start = ((), (), s32[]{:S(2)}) async-start(), calls=%async_computation.3 | async-start | bytes 2621440 | tf_op jit(solution)/shard_map/all_gather | solution.py:116
  11.2 695.8 %all-gather.19.cloned.1.call-start = ((), (), s32[]{:S(2)}) async-start(), calls=%async_computation.4 | async-start | bytes 2621440 | tf_op jit(solution)/shard_map/all_gather | solution.py:119
  11.9 698.6 %all-gather.29.cloned.1.call-start = ((), (), s32[]{:S(2)}) async-start(), calls=%async_computation.10 | async-start | bytes 1310720 | tf_op jit(solution)/shard_map/all_gather | solution.py:234
  14.5 273.4 %copy-start.20 = (f32[128]{0:T(128)}, f32[128]{0:T(128)S(1)}, u32[]{:S(2)}) copy-start(f32[128]{0:T(128)S(1)} %add_rsqrt_fusion.2) | copy-start | bytes 1540
  60.8 48.3 %copy-start.22 = (f32[128,8]{0,1:T(8,128)S(1)}, f32[128,8]{0,1:T(8,128)}, u32[]{:S(2)}) copy-start(f32[128,8]{0,1:T(8,128)} %param.42) | copy-start | bytes 12292
  60.8 48.4 %copy-start.23 = (f32[128,8]{0,1:T(8,128)S(1)}, f32[128,8]{0,1:T(8,128)}, u32[]{:S(2)}) copy-start(f32[128,8]{0,1:T(8,128)} %param.43) | copy-start | bytes 12292
  107.0 603.7 %all-gather.27.cloned.1.call-start = ((), (), s32[]{:S(2)}) async-start(), calls=%async_computation.8 | async-start | bytes 2621440 | tf_op jit(solution)/shard_map/all_gather | solution.py:123
  107.7 630.1 %reduce-scatter.2.cloned.1.call-start = ((), (), s32[]{:S(2)}) async-start(), calls=%async_computation.9 | async-start | bytes 786432 | tf_op jit(solution)/shard_map/reduce_scatter | solution.py:248
  114.7 37.5 %copy-start.18 = (bf16[128,512]{1,0:T(8,128)(2,1)S(1)}, bf16[128,512]{1,0:T(8,128)(2,1)}, u32[]{:S(2)}) copy-start(bf16[128,512]{1,0:T(8,128)(2,1)} %copy-done.17) | copy-start | bytes 393220
  114.7 37.5 %copy-start.26 = (f32[4]{0:T(128)S(1)}, f32[4]{0:T(128)}, u32[]{:S(2)}) copy-start(f32[4]{0:T(128)} %param.49) | copy-start | bytes 52
  114.7 37.7 %copy-start.13 = (pred[128,128]{0,1:T(8,128)(4,1)S(1)}, pred[128,128]{0,1:T(8,128)(4,1)}, u32[]{:S(2)}) copy-start(pred[128,128]{0,1:T(8,128)(4,1)} %broadcast_compare_fusion.1) | copy-start | bytes 49156
  369.7 11.9 %copy-start.5 = (f32[8,1,32,32]{2,3,1,0:T(8,128)S(1)}, f32[8,1,32,32]{2,3,1,0:T(8,128)}, u32[]{:S(2)}) copy-start(f32[8,1,32,32]{2,3,1,0:T(8,128)} %custom-call.7) | copy-start | bytes 98308 | tf_op jit(solution)/shard_map/while
  369.7 12.3 %copy-start.2 = (f32[32,32,8,64]{3,2,1,0:T(8,128)S(1)}, f32[32,32,8,64]{3,2,1,0:T(8,128)}, u32[]{:S(2)}) copy-start(f32[32,32,8,64]{3,2,1,0:T(8,128)} %copy-done.1) | copy-start | bytes 6291460 | tf_op jit(solution)/shard_map/while
  456.2 12.2 %copy-start.2 = (f32[32,32,8,64]{3,2,1,0:T(8,128)S(1)}, f32[32,32,8,64]{3,2,1,0:T(8,128)}, u32[]{:S(2)}) copy-start(f32[32,32,8,64]{3,2,1,0:T(8,128)} %copy-done.1) | copy-start | bytes 6291460 | tf_op jit(solution)/shard_map/while
  542.6 12.2 %copy-start.2 = (f32[32,32,8,64]{3,2,1,0:T(8,128)S(1)}, f32[32,32,8,64]{3,2,1,0:T(8,128)}, u32[]{:S(2)}) copy-start(f32[32,32,8,64]{3,2,1,0:T(8,128)} %copy-done.1) | copy-start | bytes 6291460 | tf_op jit(solution)/shard_map/while
  628.9 12.2 %copy-start.2 = (f32[32,32,8,64]{3,2,1,0:T(8,128)S(1)}, f32[32,32,8,64]{3,2,1,0:T(8,128)}, u32[]{:S(2)}) copy-start(f32[32,32,8,64]{3,2,1,0:T(8,128)} %copy-done.1) | copy-start | bytes 6291460 | tf_op jit(solution)/shard_map/while
  659.2 35.8 %copy-start.4 = (f32[8,64,64]{1,2,0:T(8,128)S(1)}, f32[8,64,64]{1,2,0:T(8,128)}, u32[]{:S(2)}) copy-start(f32[8,64,64]{1,2,0:T(8,128)} %custom-call.4) | copy-start | bytes 393220
  (26 other events, 105.9 us)
Sparse Core Ops, SparseCore 0:
  9.6 48.3 all-gather.24
  59.5 44.4 all-gather.20
  105.6 44.4 all-gather.22
  151.5 44.4 all-gather.14
  197.4 44.4 all-gather.12
  243.4 44.4 all-gather.16
  289.4 44.4 all-gather.18
  335.5 26.9 all-gather.28
  364.0 45.3 all-gather.26
  715.0 22.6 reduce-scatter.1
where the time goes:
time: 743 us; the launch traced here: 745 us
  waiting for transfers between devices  274 us (37%)
  matrix products  220 us (30%)
  other arithmetic  132 us (18%)
  local copies, waits for them, and re-layouts  50.5 us (7%)
  blocking collectives  34.5 us (5%)
  loops' own time  18.9 us (3%)
  between operations  15.1 us (2%)
    another operation x20, other arithmetic, block_pass(): jax.scipy.linalg.solve_triangular(weigh_steer + diagonal, entering, lower...  93.1 us
    dot_general x4, matrix products, block_pass(): jnp.einsum('tjhc,jhc->htj', unit_fade, steering, precision=highest)  45.6 us
    dot_general x4, matrix products, block_pass(): jnp.einsum('tjhc,jhc->htj', unit_fade, keys_c, precision=highest)  44 us
    all_gather x1, waiting for transfers between devices, local(): lax.all_gather(matrices[5], 'sp', axis=0, tiled=True)  43.5 us
    all_gather x1, waiting for transfers between devices, local(): lax.all_gather(matrices[6], 'sp', axis=0, tiled=True)  43.2 us
    all_gather x1, waiting for transfers between devices, local(): lax.all_gather(matrices[0], 'sp', axis=0, tiled=True)  42.9 us
    all_gather x1, waiting for transfers between devices, local(): lax.all_gather(matrices[2], 'sp', axis=0, tiled=True)  42.6 us
    all_gather x1, waiting for transfers between devices, local(): lax.all_gather(matrices[1], 'sp', axis=0, tiled=True)  39.7 us
  transfers between devices with their start and end apart: 10, of which 7 were waited for; matrix products, arithmetic and copies ran while one was open for 53% of the time, Pallas kernels for 0%

commit v1 on v0

--- a/solution.py
+++ b/solution.py
@@ -1,6 +1,8 @@
 import jax
 import jax.numpy as jnp
 from jax import lax
+from jax.experimental import pallas as pl
+from jax.experimental.pallas import tpu as pltpu
 from jax.sharding import PartitionSpec as P
 
 HEAD_A = 64
@@ -81,7 +83,7 @@
     return (closing, jnp.transpose(readout, (1, 0, 2)))
 
 
-def local(
+def local_positions(
     tokens,
     norm_gain,
     w_recept,
@@ -257,7 +259,315 @@
     return (mixed, row_log)
 
 
+LANES = 128
+CHUNK = 64
+TOGETHER = 4
+
+
+def dot_t(a, b, dims):
+    return lax.dot_general(a, b, (dims, ((), ())), preferred_element_type=jnp.float32)
+
+
+def split(a):
+    high = a.astype(jnp.bfloat16)
+    return high, (a - high.astype(jnp.float32)).astype(jnp.bfloat16)
+
+
+def mm(a, b, dims=((1,), (0,))):
+    a_high, a_low = split(a)
+    b_high, b_low = split(b)
+    return dot_t(a_high, b_high, dims) + (dot_t(a_high, b_low, dims) + dot_t(a_low, b_high, dims))
+
+
+NT = ((1,), (1,))
+TN = ((0,), (0,))
+
+
+def project_kernel(x_ref, *refs):
+    weights, out_ref = refs[:-1], refs[-1]
+    x = x_ref[...]
+    for i, w_ref in enumerate(weights):
+        result = jnp.dot(x, w_ref[...], preferred_element_type=jnp.float32).astype(jnp.bfloat16)
+        for s in range(out_ref.shape[0]):
+            out_ref[s, :, i * LANES : (i + 1) * LANES] = result[:, s * LANES : (s + 1) * LANES]
+
+
+def project(x, weights, shares):
+    return pl.pallas_call(
+        project_kernel,
+        out_shape=jax.ShapeDtypeStruct((shares, x.shape[0], LANES * len(weights)), jnp.bfloat16),
+    )(x, *weights)
+
+
+def per_head_sum(a, first):
+    left = jnp.sum(jnp.where(first, a, 0.0), axis=1, keepdims=True)
+    right = jnp.sum(jnp.where(first, 0.0, a), axis=1, keepdims=True)
+    return jnp.where(first, left, right)
+
+
+def state_kernel(
+    rkv_ref, low_ref, up_ref, vec_ref, out_ref, m_ref, b_ref, p_ref, n_ref, log_ref, mix_ref, unit_ref
+):
+    rows = rkv_ref.shape[0]
+    first = lax.broadcasted_iota(jnp.int32, (1, LANES), 1) < HEAD_A
+    low = low_ref[...]
+    rank = up_ref.shape[0] // 2
+    decay_low = low[:, :rank].astype(jnp.bfloat16)
+    rate_low = low[:, rank : 2 * rank].astype(jnp.bfloat16)
+    extra = low[:, 2 * rank :]
+    shift = jnp.where(first, extra[:, 0:1], extra[:, 1:2])
+    jolt = jnp.where(first, extra[:, 2:3], extra[:, 3:4])
+    preact = vec_ref[0:1] + jnp.dot(decay_low, up_ref[:rank], preferred_element_type=jnp.float32) + shift
+    log_ref[...] = -jnp.exp(-0.5) * jax.nn.sigmoid(preact) - jolt
+    mix_ref[...] = jax.nn.sigmoid(
+        vec_ref[1:2] + jnp.dot(rate_low, up_ref[rank:], preferred_element_type=jnp.float32)
+    )
+    keys_all = rkv_ref[:, LANES : 2 * LANES].astype(jnp.float32)
+    unit_ref[...] = keys_all * lax.rsqrt(per_head_sum(keys_all * keys_all, first) + 1e-06)
+
+    row = lax.broadcasted_iota(jnp.int32, (LANES, LANES), 0)
+    col = lax.broadcasted_iota(jnp.int32, (LANES, LANES), 1)
+    same_head = (row // CHUNK) == (col // CHUNK)
+    strict = same_head & (row > col)
+    inclusive = same_head & (row >= col)
+    eye = (row == col).astype(jnp.float32)
+    tri = (
+        lax.broadcasted_iota(jnp.int32, (CHUNK, CHUNK), 0)
+        >= lax.broadcasted_iota(jnp.int32, (CHUNK, CHUNK), 1)
+    ).astype(jnp.bfloat16)
+
+    def stack(a):
+        return jnp.concatenate([jnp.where(first, a, 0.0), jnp.where(first, 0.0, a)], axis=0)
+
+    def inverse(lower):
+        near = (row // 16) == (col // 16)
+        power = jnp.where(near, lower, 0.0)
+        result = eye - power
+        for _ in range(3):
+            power = mm(power, power)
+            result = result + mm(result, power)
+        size = 16
+        while size < CHUNK:
+            joining = (row // size != col // size) & (row // (2 * size) == col // (2 * size))
+            corner = jnp.where(joining, lower, 0.0)
+            result = result - mm(mm(result, corner), result)
+            size = 2 * size
+        return result
+
+    def prepare(c):
+        at = pl.ds(pl.multiple_of(c * CHUNK, CHUNK), CHUNK)
+        logs = log_ref[at]
+        log_high, log_low = split(logs)
+        log_last = (logs - log_high.astype(jnp.float32) - log_low.astype(jnp.float32)).astype(jnp.bfloat16)
+        dims = ((1,), (0,))
+        totals = dot_t(tri, log_high, dims) + (dot_t(tri, log_low, dims) + dot_t(tri, log_last, dims))
+        preceding = totals - logs
+        middle = totals[CHUNK // 2 - 1 : CHUNK // 2]
+        final = totals[CHUNK - 1 : CHUNK]
+        recept = rkv_ref[at, 0:LANES].astype(jnp.float32)
+        keys = rkv_ref[at, LANES : 2 * LANES].astype(jnp.float32)
+        values = stack(rkv_ref[at, 2 * LANES : 3 * LANES].astype(jnp.float32))
+        unit = unit_ref[at]
+        steer = unit * mix_ref[at]
+        growth = jnp.exp(middle - totals)
+        unit_in = stack(unit * jnp.exp(preceding - middle))
+        recept_in = stack(recept * jnp.exp(totals - middle))
+        keys_out = stack(keys * growth)
+        steer_out = stack(steer * growth)
+        weigh_keys = jnp.where(strict, mm(unit_in, keys_out, NT), 0.0)
+        weigh_steer = jnp.where(strict, mm(unit_in, steer_out, NT), 0.0)
+        read_keys = jnp.where(inclusive, mm(recept_in, keys_out, NT), 0.0)
+        read_steer = jnp.where(inclusive, mm(recept_in, steer_out, NT), 0.0)
+        solved = inverse(weigh_steer)
+        fade = jnp.exp(final - totals)
+        keys_end = stack(keys * fade)
+        steer_end = stack(steer * fade)
+        q = mm(solved, stack(unit * jnp.exp(preceding)))
+        u = mm(solved, mm(weigh_keys, values))
+        m_ref[c] = eye * jnp.exp(final) - mm(steer_end, q, TN)
+        b_ref[c] = mm(keys_end, values, TN) - mm(steer_end, u, TN)
+        p_ref[c] = stack(recept * jnp.exp(totals)) - mm(read_steer, q)
+        n_ref[c] = mm(read_keys, values) - mm(read_steer, u)
+
+    chunks = rows // CHUNK
+    together = TOGETHER if chunks % TOGETHER == 0 else 1
+
+    def lap(i, nothing):
+        for k in range(together):
+            prepare(i * together + k)
+        return nothing
+
+    lax.fori_loop(0, chunks // together, lap, 0)
+
+    def advance(c, state):
+        reads = mm(p_ref[c], state) + n_ref[c]
+        out_ref[pl.ds(pl.multiple_of(c * CHUNK, CHUNK), CHUNK), :] = reads[:CHUNK] + reads[CHUNK:]
+        return mm(m_ref[c], state) + b_ref[c]
+
+    lax.fori_loop(0, chunks, advance, jnp.zeros((LANES, LANES), jnp.float32))
+    reads = out_ref[...]
+    centered = reads - per_head_sum(reads, first) * (1.0 / HEAD_A)
+    variance = per_head_sum(centered * centered, first) * (1.0 / HEAD_A)
+    out_ref[...] = centered * lax.rsqrt(variance + 0.00064) * vec_ref[2:3]
+
+
+def state_mixer(rkv, low, up, vectors):
+    rows = rkv.shape[0]
+    square = pltpu.VMEM((rows // CHUNK, LANES, LANES), jnp.float32)
+    full = pltpu.VMEM((rows, LANES), jnp.float32)
+    return pl.pallas_call(
+        state_kernel,
+        out_shape=jax.ShapeDtypeStruct((rows, LANES), jnp.float32),
+        scratch_shapes=[square, square, square, square, full, full, full],
+    )(rkv, low, up, vectors)
+
+
+def silu(a):
+    return a * jax.nn.sigmoid(a)
+
+
+def stick_kernel(rest_ref, normal_ref, offset_ref, out_ref):
+    rows = rest_ref.shape[0]
+    factor = HEAD_B ** (-0.5)
+    row = lax.broadcasted_iota(jnp.int32, (LANES, LANES), 0)
+    col = lax.broadcasted_iota(jnp.int32, (LANES, LANES), 1)
+    causal = col < row
+    later = (row > col).astype(jnp.bfloat16)
+    gate_a = rest_ref[:, 3 * LANES : 4 * LANES].astype(jnp.float32)
+    out_ref[:, 0:LANES] = (normal_ref[...] * silu(gate_a)).astype(jnp.bfloat16)
+    offset = offset_ref[0:1, :]
+    dims = ((1,), (0,))
+    for i in range(rows // LANES):
+        at = slice(i * LANES, (i + 1) * LANES)
+        query = rest_ref[at, 0:LANES]
+        survive = jnp.zeros((LANES, 1), jnp.float32)
+        weight_sum = jnp.zeros((LANES, 1), jnp.float32)
+        attended = jnp.zeros((LANES, LANES), jnp.float32)
+        for j in range(i, -1, -1):
+            there = slice(j * LANES, (j + 1) * LANES)
+            scores = dot_t(query, rest_ref[there, LANES : 2 * LANES], NT) * factor + offset
+            keep = -(jnp.maximum(scores, 0.0) + jnp.log1p(jnp.exp(-jnp.abs(scores))))
+            taken = scores + keep
+            if i == j:
+                keep = jnp.where(causal, keep, 0.0)
+            keep_high, keep_low = split(keep)
+            after = dot_t(keep_high, later, dims) + dot_t(keep_low, later, dims)
+            weights = jnp.exp(taken + after + survive)
+            if i == j:
+                weights = jnp.where(causal, weights, 0.0)
+            survive = survive + jnp.sum(keep, axis=1, keepdims=True)
+            weight_sum = weight_sum + jnp.sum(weights, axis=1, keepdims=True)
+            attended = attended + dot_t(
+                weights.astype(jnp.bfloat16), rest_ref[there, 2 * LANES : 3 * LANES], dims
+            )
+        gate_b = rest_ref[at, 4 * LANES : 5 * LANES].astype(jnp.float32)
+        out_ref[at, LANES : 2 * LANES] = (attended * silu(gate_b)).astype(jnp.bfloat16)
+        row_log = jnp.log(jnp.maximum(weight_sum, 0.01))
+        log_high = row_log.astype(jnp.bfloat16).astype(jnp.float32)
+        log_low = (row_log - log_high).astype(jnp.bfloat16).astype(jnp.float32)
+        out_ref[at, 2 * LANES : 3 * LANES] = jnp.where(
+            col == 0, log_high, jnp.where(col == 1, log_low, 0.0)
+        ).astype(jnp.bfloat16)
+
+
+def stick_mixer(rest, normal, offset):
+    return pl.pallas_call(
+        stick_kernel,
+        out_shape=jax.ShapeDtypeStruct((rest.shape[0], 3 * LANES), jnp.bfloat16),
+    )(rest, normal, offset)
+
+
+def local_heads(
+    tokens,
+    norm_gain,
+    w_recept,
+    w_key_a,
+    w_value_a,
+    w_gate_a,
+    decay_down_weight,
+    decay_up_weight,
+    rate_down_weight,
+    rate_up_weight,
+    decay_base,
+    rate_base,
+    rate_shift,
+    jolts,
+    group_gain,
+    w_query_b,
+    w_key_b,
+    w_value_b,
+    w_gate_b,
+    score_offset,
+    w_out_a,
+    w_out_b,
+):
+    shares, index = lax.axis_size("sp"), lax.axis_index("sp")
+    gathered = lax.all_gather(tokens, "tp", axis=1, tiled=True)
+    floats = gathered.astype(jnp.float32)
+    normed = (
+        floats * lax.rsqrt(jnp.mean(floats * floats, axis=1, keepdims=True) + 1e-06) * norm_gain
+    ).astype(jnp.bfloat16)
+    rows = normed.shape[0]
+    features = lax.all_to_all(normed, "sp", split_axis=1, concat_axis=0, tiled=True)
+    decay_low = jnp.tanh(jnp.dot(normed, decay_down_weight, preferred_element_type=jnp.float32))
+    rate_low = jnp.dot(normed, rate_down_weight, preferred_element_type=jnp.float32)
+    small = jnp.concatenate([decay_low, rate_low, rate_shift, jolts], axis=1)
+    small = lax.all_gather(small, "sp", axis=0, tiled=True)
+    rank = decay_low.shape[1]
+    local_a = rate_shift.shape[1]
+    own_a = local_a // shares
+
+    def own(array, size, start=0):
+        return lax.dynamic_slice_in_dim(array, start + index * size, size, axis=array.ndim - 1)
+
+    low = jnp.concatenate(
+        [
+            small[:, : 2 * rank],
+            own(small, own_a, 2 * rank),
+            own(small, own_a, 2 * rank + local_a),
+        ],
+        axis=1,
+    )
+    up = own(jnp.concatenate([decay_up_weight, rate_up_weight], axis=0), LANES)
+    vectors = own(jnp.stack([decay_base, rate_base, group_gain]), LANES)
+    offset = jnp.broadcast_to(own(score_offset, score_offset.shape[0] // shares), (8, LANES))
+
+    part_a = project(features, (w_recept, w_key_a, w_value_a), shares)
+    rkv = lax.psum_scatter(part_a, "sp", scatter_dimension=0, tiled=True)[0]
+    part_b = project(features, (w_query_b, w_key_b, w_value_b, w_gate_a, w_gate_b), shares)
+    rest = lax.psum_scatter(part_b, "sp", scatter_dimension=0, tiled=True)[0]
+    normal = state_mixer(rkv, low, up, vectors)
+    both = stick_mixer(rest, normal, offset)
+    back = lax.all_to_all(
+        both.reshape(shares, rows, 3 * LANES), "sp", split_axis=0, concat_axis=0, tiled=True
+    )
+    back = jnp.transpose(back, (1, 0, 2))
+    mixed_a = back[:, :, :LANES].reshape(rows, -1)
+    mixed_b = back[:, :, LANES : 2 * LANES].reshape(rows, -1)
+    logs = back[:, :, 2 * LANES : 2 * LANES + 2].astype(jnp.float32)
+    row_log = logs[:, :, 0] + logs[:, :, 1]
+    mixed = lax.psum_scatter(
+        (
+            jnp.dot(mixed_a, w_out_a, preferred_element_type=jnp.float32)
+            + jnp.dot(mixed_b, w_out_b, preferred_element_type=jnp.float32)
+        ).astype(jnp.bfloat16),
+        "tp",
+        scatter_dimension=0,
+        tiled=True,
+    )
+    return (mixed, row_log)
+
+
 def solution(mesh):
+    def chosen(*arrays):
+        width = arrays[2].shape[1]
+        shares = mesh.shape["sp"]
+        whole_heads = width == shares * LANES and arrays[15].shape[1] == width
+        rows = arrays[0].shape[0]
+        if whole_heads and rows % LANES == 0:
+            return local_heads(*arrays)
+        return local_positions(*arrays)
+
     in_specs = (
         P(("fs", "sp"), "tp"),
         P(),
@@ -283,4 +593,4 @@
         P("tp", None),
     )
     out_specs = (P(("fs", "sp", "tp"), None), P(("fs", "sp"), "tp"))
-    return jax.shard_map(local, mesh=mesh, in_specs=in_specs, out_specs=out_specs, check_vma=False)
+    return jax.shard_map(chosen, mesh=mesh, in_specs=in_specs, out_specs=out_specs, check_vma=False)

time: 743 us -> 170 us (0.23)
  waiting for transfers between devices: 274 us -> 49.5 us
  matrix products: 220 us -> 2.32 us
  other arithmetic: 132 us -> 4 us
  local copies, waits for them, and re-layouts: 50.5 us -> 5.35 us
  Pallas kernels: 0 us -> 34.2 us
  blocking collectives: 34.5 us -> 60.2 us
  loops' own time: 18.9 us -> 0 us
    all_gather x9 -> x0, waiting for transfers between devices: 247 us -> none  [the longest x1 43.5 us: local(): lax.all_gather(matrices[5], 'sp', axis=0, tiled=True)]
    dot_general x61 -> x4, matrix products: 219 us -> 2.32 us  [the longest x1 1.26 us: local_heads(): jnp.dot(mixed_b, w_out_b, preferred_element_type=jnp.float32)]
    another operation x26 -> x1, other arithmetic: 97.9 us -> 0.66 us  [local_heads(): vectors = own(jnp.stack([decay_base, rate_base, group_gain]), LANES)]
    all_to_all x0 -> x2, blocking collectives: none -> 35.8 us  [the longest x1 20.9 us: local_heads(): lax.all_to_all(normed, 'sp', split_axis=1, concat_axis=0, tiled=True)]
    pallas_call x0 -> x4, Pallas kernels: none -> 34.2 us  [the longest x1 21.9 us: state_mixer(): pl.pallas_call(state_kernel, out_shape=jax.ShapeDtypeStruct((rows, LANES)...]
    reduce_scatter x1 -> x3, waiting for transfers between devices: 22.3 us -> 49.4 us  [the longest x1 31.7 us: local_heads(): rest = lax.psum_scatter(part_b, 'sp', scatter_dimension=0, tiled=True)[0]]
    another operation x6 -> x0, loops' own time: 18.9 us -> none  [the longest x1 18.6 us: local(): lax.scan(block_pass, jnp.concatenate([identity, zeros_state], axis=1), in...]
    mul x10 -> x0, other arithmetic: 18 us -> none  [the longest x4 13 us: block_pass(): read_fade = fading * (recept_c * jnp.exp(logs_step))[:, None]]
  transfers between devices with their start and end apart: 10 -> 3, of which waited for: 7 -> 3; matrix products, arithmetic and copies ran while one was open for 53% -> 3% of each run, Pallas kernels for 0% -> 16%
where the time goes in v1:
time: 170 us; the launch traced here: 169 us
  blocking collectives  60.2 us (35%)
  waiting for transfers between devices  49.5 us (29%)
  Pallas kernels  34.2 us (20%)
  between operations  13.9 us (8%)
  local copies, waits for them, and re-layouts  5.35 us (3%)
  other arithmetic  4 us (2%)
  matrix products  2.32 us (1%)
    reduce_scatter x1, waiting for transfers between devices, local_heads(): rest = lax.psum_scatter(part_b, 'sp', scatter_dimension=0, tiled=True)[0]  31.7 us
    pallas_call x1, Pallas kernels, state_mixer(): pl.pallas_call(state_kernel, out_shape=jax.ShapeDtypeStruct((rows, LANES)...  21.9 us
    all_gather x1, blocking collectives, local_heads(): small = lax.all_gather(small, 'sp', axis=0, tiled=True)  21.8 us
    all_to_all x1, blocking collectives, local_heads(): lax.all_to_all(normed, 'sp', split_axis=1, concat_axis=0, tiled=True)  20.9 us
    all_to_all x1, blocking collectives, local_heads(): lax.all_to_all(both.reshape(shares, rows, 3 * LANES), 'sp', split_axis=0,...  14.8 us
    reduce_scatter x1, waiting for transfers between devices, local_heads(): rkv = lax.psum_scatter(part_a, 'sp', scatter_dimension=0, tiled=True)[0]  11.5 us
    pallas_call x2, Pallas kernels, project(): pl.pallas_call(project_kernel, out_shape=jax.ShapeDtypeStruct((shares, x....  8.57 us
    reduce_scatter x1, waiting for transfers between devices, local_heads(): lax.psum_scatter((jnp.dot(mixed_a, w_out_a, preferred_element_type=jnp.fl...  6.2 us
  transfers between devices with their start and end apart: 3, of which 3 were waited for; matrix products, arithmetic and copies ran while one was open for 3% of the time, Pallas kernels for 16%

profile of v1, /device:TPU:0, one launch (start us, length us, event | category | flops | bytes accessed | tf_op | source)
XLA Modules:
  0.0 169.5 jit_solution(14268552995113934831)
XLA Ops:
  7.2 2.6 %all_gather.6 = bf16[128,2048]{1,0:T(8,128)(2,1)S(1)} all-gather(bf16[128,1024]{1,0:T(8,128)(2,1)} %param.22), channel_id=1, replica_groups=mesh['sp'=4,'fs'=4,'tp'=2] {'tp'}, dimensions={1}, use_global_device_ids=true | all-gather | bytes 786432 | tf_op jit(solution)/shard_map/all_gather | solution.py:505
  10.1 0.9 fusion.3
  11.0 20.9 %all_to_all.24 = bf16[128,4,512]{2,0,1:T(8,128)(2,1)} all-to-all(bf16[128,4,512]{2,0,1:T(8,128)(2,1)S(1)} %bitcast.29), channel_id=1, replica_groups=mesh['sp'=4,'fs'=4,'tp'=2] {'sp'}, dimensions={1} | all-to-all | bytes 1048576 | tf_op jit(solution)/shard_map/all_to_all | solution.py:511
  31.9 3.7 %shard_map.222 = bf16[4,512,384]{2,1,0:T(8,128)(2,1)} custom-call(bf16[512,512]{1,0:T(8,128)(2,1)} %bitcast.27, bf16[512,512]{1,0:T(8,128)(2,1)} %refs_0_.3, bf16[512,512]{1,0:T(8,128)(2,1)} %refs_1_.3, bf16[512,512]{1,0:T(8,128)(2,1)} %refs_2_.3), custom_call_target="tpu_custom_call" | custom-call | tf_op jit(solution)/shard_map/pallas_call | solution.py:296
  35.7 4.9 %shard_map.221 = bf16[4,512,640]{2,1,0:T(8,128)(2,1)} custom-call(bf16[512,512]{1,0:T(8,128)(2,1)} %bitcast.28, bf16[512,512]{1,0:T(8,128)(2,1)} %refs_0_.2, bf16[512,512]{1,0:T(8,128)(2,1)} %refs_1_.2, bf16[512,512]{1,0:T(8,128)(2,1)} %refs_2_.2, bf16[512,512]{1,0:T(8,128)(2,1)} %refs_3_.1, bf16[512,512]{1,0:T(8,128)(2,1)} %refs_4_.1), custom_call_target="tpu_custom_call" | custom-call | tf_op jit(solution)/shard_map/pallas_call | solution.py:296
  40.7 0.5 copy-done.6
  41.6 0.3 convolution_tanh_fusion
  42.4 21.8 %all_gather.7 = f32[512,144]{1,0:T(8,128)S(1)} all-gather(f32[128,144]{1,0:T(8,128)S(1)} %pad_maximum_fusion.1), channel_id=1, replica_groups=mesh['sp'=4,'fs'=4,'tp'=2] {'sp'}, dimensions={0}, use_global_device_ids=true | all-gather | bytes 368640 | tf_op jit(solution)/shard_map/all_gather | solution.py:515
  64.2 0.6 dynamic_slice.21
  64.8 0.7 fusion.6.vec_ref
  65.5 0.6 fusion.4.up_ref
  66.3 0.9 pad_maximum_fusion.low_ref
  67.2 11.5 %reduce-scatter.6.cloned.1.call-done = bf16[1,512,384]{2,1,0:T(8,128)(2,1)} async-done(((bf16[4,512,384]{2,1,0:T(8,128)(2,1)}), bf16[1,512,384]{2,1,0:T(8,128)(2,1)}) %reduce-scatter.6.cloned.1.call-update) | async-done | bytes 393232 | tf_op jit(solution)/shard_map/reduce_scatter | solution.py:536
  78.8 21.9 %shard_map.223.normal_ref = f32[512,128]{1,0:T(8,128)} custom-call(bf16[512,384]{1,0:T(8,128)(2,1)} %bitcast.36, f32[512,132]{1,0:T(8,128)} %pad_maximum_fusion.low_ref, bf16[128,128]{1,0:T(8,128)(2,1)} %fusion.4.up_ref, f32[3,128]{1,0:T(4,128)} %fusion.6.vec_ref), custom_call_target="tpu_custom_call" | custom-call | tf_op jit(solution)/shard_map/pallas_call | solution.py:418
  100.6 31.7 %reduce-scatter.4.cloned.1.call-done = bf16[1,512,640]{2,1,0:T(8,128)(2,1)} async-done(((bf16[4,512,640]{2,1,0:T(8,128)(2,1)}), bf16[1,512,640]{2,1,0:T(8,128)(2,1)}) %reduce-scatter.4.cloned.1.call-update) | async-done | bytes 655376 | tf_op jit(solution)/shard_map/reduce_scatter | solution.py:538
  132.3 1.2 broadcast_in_dim.2.offset_ref
  133.5 3.7 %shard_map.224 = bf16[512,384]{1,0:T(8,128)(2,1)} custom-call(bf16[512,640]{1,0:T(8,128)(2,1)} %bitcast.33, f32[512,128]{1,0:T(8,128)} %shard_map.223.normal_ref, f32[8,128]{1,0:T(8,128)} %broadcast_in_dim.2.offset_ref), custom_call_target="tpu_custom_call" | custom-call | tf_op jit(solution)/shard_map/pallas_call | solution.py:474
  137.2 1.2 copy.41
  138.5 14.8 %all_to_all.25 = bf16[4,128,384]{1,2,0:T(8,128)(2,1)S(1)} all-to-all(bf16[4,128,384]{1,2,0:T(8,128)(2,1)S(1)} %copy.41), channel_id=1, replica_groups=mesh['sp'=4,'fs'=4,'tp'=2] {'sp'}, dimensions={0} | all-to-all | bytes 786432 | tf_op jit(solution)/shard_map/all_to_all | solution.py:541
  153.3 0.5 fusion.9
  153.8 1.1 copy-done.1
  154.9 1.3 fusion
  156.2 0.6 slice_add_fusion
  156.8 6.2 %reduce-scatter.8.cloned.1.call-done = bf16[64,2048]{1,0:T(8,128)(2,1)} async-done(((bf16[128,2048]{1,0:T(8,128)(2,1)}), bf16[64,2048]{1,0:T(8,128)(2,1)}) %reduce-scatter.8.cloned.1.call-update) | async-done | bytes 262160 | tf_op jit(solution)/shard_map/reduce_scatter | solution.py:549
  (40 shorter events, 1.5 us)
Async XLA Ops:
  7.2 146.2 %copy-start = (bf16[512,2048]{1,0:T(8,128)(2,1)S(1)}, bf16[512,2048]{1,0:T(8,128)(2,1)}, u32[]{:S(2)}) copy-start(bf16[512,2048]{1,0:T(8,128)(2,1)} %param.42) | copy-start | bytes 6291460
  7.2 71.6 %reduce-scatter.6.cloned.1.call-start = ((), (), s32[]{:S(2)}) async-start(), calls=%async_computation.6 | async-start | bytes 1966080 | tf_op jit(solution)/shard_map/reduce_scatter | solution.py:536
  35.6 96.6 %reduce-scatter.4.cloned.1.call-start = ((), (), s32[]{:S(2)}) async-start(), calls=%async_computation.5 | async-start | bytes 3276800 | tf_op jit(solution)/shard_map/reduce_scatter | solution.py:538
  40.6 0.7 copy-start.6
  40.6 0.8 copy-start.7
  40.6 1.0 copy-start.2
  40.6 1.4 copy-start.3
  40.6 23.6 %copy-start.11 = (f32[4]{0:T(128)S(1)}, f32[4]{0:T(128)}, u32[]{:S(2)}) copy-start(f32[4]{0:T(128)} %param.41) | copy-start | bytes 52
  40.6 24.2 %copy-start.8 = (f32[512]{0:T(512)S(1)}, f32[512]{0:T(512)}, u32[]{:S(2)}) copy-start(f32[512]{0:T(512)} %param.32) | copy-start | bytes 6148
  40.6 24.2 %copy-start.9 = (f32[512]{0:T(512)S(1)}, f32[512]{0:T(512)}, u32[]{:S(2)}) copy-start(f32[512]{0:T(512)} %param.33) | copy-start | bytes 6148
  40.7 24.1 %copy-start.10 = (f32[512]{0:T(512)S(1)}, f32[512]{0:T(512)}, u32[]{:S(2)}) copy-start(f32[512]{0:T(512)} %param.36) | copy-start | bytes 6148
  40.7 24.8 %copy-start.4 = (bf16[64,512]{1,0:T(8,128)(2,1)S(1)}, bf16[64,512]{1,0:T(8,128)(2,1)}, u32[]{:S(2)}) copy-start(bf16[64,512]{1,0:T(8,128)(2,1)} %param.29) | copy-start | bytes 196612
  40.7 24.8 %copy-start.5 = (bf16[64,512]{1,0:T(8,128)(2,1)S(1)}, bf16[64,512]{1,0:T(8,128)(2,1)}, u32[]{:S(2)}) copy-start(bf16[64,512]{1,0:T(8,128)(2,1)} %param.31) | copy-start | bytes 196612
  40.7 122.3 %reduce-scatter.8.cloned.1.call-start = ((), (), s32[]{:S(2)}) async-start(), calls=%async_computation.7 | async-start | bytes 786432 | tf_op jit(solution)/shard_map/reduce_scatter | solution.py:549
  153.3 1.6 copy-start.1
Sparse Core Ops, SparseCore 0:
  35.8 42.9 reduce-scatter.5
  81.1 51.1 reduce-scatter.3
  156.3 6.6 reduce-scatter.7
